TPU v7x, 32 devices: a whole 2x2x4 slice. The times are simulated.
32 devices in a mesh: sp: 8 (over z, x), dp: 4 (over y, core).
Axes of the slice: x: 2, y: 2, z: 4, core: 2. Of those that a mesh axis runs over, the one named last changes fastest.
Arguments:
- resid: bfloat16 [4, 2048, 2048], P('dp', 'sp'), may hold values from -4 to 4
- query: bfloat16 [4, 2048, 2048], P('dp', 'sp'), may hold values from -6 to 6
- keys: bfloat16 [4, 2048, 512], P('dp', 'sp'), may hold values from -6 to 6
- values: bfloat16 [4, 2048, 512], P('dp', 'sp'), may hold values from -6 to 6
- q_gain: float32 [128], replicated, may hold values from 0.7 to 5
- k_gain: float32 [128], replicated, may hold values from 0.7 to 5
- out_weight: bfloat16 [2048, 2048], P('dp'), may hold values from -0.5 to 0.5
- norm_gain: float32 [2048], replicated, may hold values from 0.1 to 1.9
- route_ids: int32 [4, 2048, 2], P('dp', 'sp'), may hold values from 0 to 31, all different within a row; in each aligned block of 256 rows (0 to 255, 256 to 511, ..., all dimensions but the last counted through in order) at most 24 rows name the same one
- route_weight: float32 [4, 2048, 2], P('dp', 'sp'), may hold values from 0.2 to 1
- expert_gate: bfloat16 [32, 2048, 1024], P(('sp', 'dp')), may hold values from -0.125 to 0.125
- expert_up: bfloat16 [32, 2048, 1024], P(('sp', 'dp')), may hold values from -0.125 to 0.125
- expert_down: bfloat16 [32, 1024, 2048], P(('sp', 'dp')), may hold values from -0.1875 to 0.1875
Outputs:
- layer_out: bfloat16 [4, 2048, 2048], P('dp', 'sp')
Inputs may be any that keep to these rules, and one draw needn't show every extreme that they name: `route_ids`: each row names 2 different experts. In the rows of one device no expert is named more than 24 times, and in some devices some expert is named exactly 24 times.
All inputs are finite; a program needn't handle non-finite values.
Results may differ from a plain program's by a relative error of at most 0.0095.
The roundings to bfloat16 on the way count: a program that leaves them out, or rounds other values in their place, can miss the bound.
Values may be sent and summed in bfloat16 or wider, within the bound.
A program may use at most 128 MiB of HBM per device.

v0:
```python
import jax
import jax.numpy as jnp
from jax import lax
from jax.sharding import PartitionSpec as P

GRID_W = 64


EPSILON = 1e-06
THETA = 10000.0
LIMIT = 7.0
SLOPE = 1.702


def turn_half(matrix, places):
    half_width = matrix.shape[-1] // 2
    inverse = THETA ** (-jnp.arange(half_width, dtype=jnp.float32) / half_width)
    angles = places.astype(jnp.float32)[:, None] * inverse[None, :]
    cosine = jnp.cos(angles)[:, None, :]
    sine_part = jnp.sin(angles)[:, None, :]
    leading = matrix[..., :half_width]
    second = matrix[..., half_width:]
    return jnp.concatenate(
        [leading * cosine - second * sine_part, second * cosine + leading * sine_part], axis=-1
    )


def prepare(projected_rows, gain_vector, head_count, places):
    matrix = projected_rows.astype(jnp.float32).reshape(projected_rows.shape[0], head_count, -1)
    matrix = (
        matrix
        * lax.rsqrt(jnp.mean(matrix * matrix, axis=-1, keepdims=True) + EPSILON)
        * gain_vector
    )
    middle = matrix.shape[-1] // 2
    turned = jnp.concatenate(
        [
            turn_half(matrix[..., :middle], places // GRID_W),
            turn_half(matrix[..., middle:], places % GRID_W),
        ],
        axis=-1,
    )
    return turned.astype(jnp.bfloat16)


def attend(head_query, head_key, head_value):
    length, local_heads, head_dim = head_query.shape
    local_kv = head_key.shape[1]
    group_size = local_heads // local_kv
    block_rows = min(512, length)
    scaling = head_dim ** (-0.5)
    query_blocks = head_query.reshape(
        length // block_rows, block_rows, local_kv, group_size, head_dim
    )

    def one_block(query_block):
        scores = (
            jnp.einsum("qkgd,skd->kgqs", query_block, head_key, preferred_element_type=jnp.float32)
            * scaling
        )
        lifted = jnp.exp(scores - jnp.max(scores, axis=-1, keepdims=True))
        attn_weights = (lifted / jnp.sum(lifted, axis=-1, keepdims=True)).astype(jnp.bfloat16)
        return jnp.einsum(
            "kgqs,skd->qkgd", attn_weights, head_value, preferred_element_type=jnp.float32
        ).astype(jnp.bfloat16)

    return lax.map(one_block, query_blocks).reshape(length, local_heads, head_dim)


def apply_expert(batch, gate_matrix, up_matrix, down_matrix):
    flat_rows = batch.reshape(-1, batch.shape[-1])
    gated = jnp.minimum(jnp.dot(flat_rows, gate_matrix, preferred_element_type=jnp.float32), LIMIT)
    linear = jnp.clip(
        jnp.dot(flat_rows, up_matrix, preferred_element_type=jnp.float32), -LIMIT, LIMIT
    )
    active = (gated * jax.nn.sigmoid(SLOPE * gated) * (linear + 1.0)).astype(jnp.bfloat16)
    return (
        jnp.dot(active, down_matrix, preferred_element_type=jnp.float32)
        .astype(jnp.bfloat16)
        .reshape(batch.shape)
    )


def per_device(
    resid,
    query,
    keys,
    values,
    q_gain,
    k_gain,
    out_weight,
    norm_gain,
    route_ids,
    route_weight,
    expert_gate,
    expert_up,
    expert_down,
):
    span_devices = lax.axis_size("sp")
    experts_total = span_devices * lax.axis_size("dp")
    tok_rows = resid.shape[1]
    model_width = resid.shape[2]
    head_dim = q_gain.shape[0]
    q_heads = query.shape[2] // head_dim
    kv_heads = keys.shape[2] // head_dim
    repeat_count = max(kv_heads, span_devices) // kv_heads
    places = lax.axis_index("sp") * tok_rows + jnp.arange(tok_rows, dtype=jnp.int32)
    query_turned = prepare(query[0], q_gain, q_heads, places)
    key_turned = jnp.repeat(prepare(keys[0], k_gain, kv_heads, places), repeat_count, axis=1)
    value_heads = jnp.repeat(values[0].reshape(tok_rows, kv_heads, head_dim), repeat_count, axis=1)
    head_query, head_key, head_value = (
        lax.all_to_all(query_turned, "sp", split_axis=1, concat_axis=0, tiled=True),
        lax.all_to_all(key_turned, "sp", split_axis=1, concat_axis=0, tiled=True),
        lax.all_to_all(value_heads, "sp", split_axis=1, concat_axis=0, tiled=True),
    )
    head_out = attend(head_query, head_key, head_value)
    token_out = lax.all_to_all(head_out, "sp", split_axis=0, concat_axis=1, tiled=True).reshape(
        tok_rows, q_heads * head_dim
    )
    projected = jnp.dot(
        token_out,
        lax.all_gather(out_weight, "dp", axis=0, tiled=True),
        preferred_element_type=jnp.float32,
    )
    updated = (resid[0].astype(jnp.float32) + projected).astype(jnp.bfloat16)
    widened = updated.astype(jnp.float32)
    normed = (
        widened
        * lax.rsqrt(jnp.mean(widened * widened, axis=-1, keepdims=True) + EPSILON)
        * norm_gain
    ).astype(jnp.bfloat16)
    top_count = route_ids.shape[2]
    capacity = max(2, 3 * tok_rows * top_count // (2 * experts_total))
    chosen = route_ids[0].reshape(-1)
    onehot = (chosen[:, None] == jnp.arange(experts_total, dtype=jnp.int32)[None, :]).astype(
        jnp.int32
    )
    earlier = jnp.sum((jnp.cumsum(onehot, axis=0) - onehot) * onehot, axis=1)
    target = chosen * capacity + earlier
    sources = jnp.arange(tok_rows * top_count, dtype=jnp.int32) // top_count
    slot_table = jnp.full((experts_total * capacity,), tok_rows, jnp.int32).at[target].set(sources)
    padded = jnp.concatenate([normed, jnp.zeros((1, model_width), jnp.bfloat16)], axis=0)
    outgoing = padded[slot_table].reshape(experts_total, capacity, model_width)
    answered = apply_expert(
        lax.all_to_all(outgoing, ("sp", "dp"), split_axis=0, concat_axis=0, tiled=True),
        expert_gate[0],
        expert_up[0],
        expert_down[0],
    )
    returned = lax.all_to_all(answered, ("sp", "dp"), split_axis=0, concat_axis=0, tiled=True)
    results = returned.reshape(experts_total * capacity, model_width)[target]
    weighted = results.astype(jnp.float32) * route_weight[0].reshape(-1)[:, None]
    combined = jnp.sum(weighted.reshape(tok_rows, top_count, model_width), axis=1)
    return (widened + combined).astype(jnp.bfloat16)[None]


def solution(mesh):
    placed = (
        P("dp", "sp", None),
        P("dp", "sp", None),
        P("dp", "sp", None),
        P("dp", "sp", None),
        P(),
        P(),
        P("dp", None),
        P(),
        P("dp", "sp", None),
        P("dp", "sp", None),
        P(("sp", "dp"), None, None),
        P(("sp", "dp"), None, None),
        P(("sp", "dp"), None, None),
    )
    return jax.shard_map(
        per_device, mesh=mesh, in_specs=placed, out_specs=P("dp", "sp", None), check_vma=False
    )
```

profile of v0, /device:TPU:0, one launch (start us, length us, event | category | flops | bytes accessed | tf_op | source)
XLA Modules:
  0.0 339.7 jit_solution(17231066613141276203)
XLA Ops:
  12.4 7.3 %all-to-all-start.1 = ((bf16[256,8,128]{2,0,1:T(8,128)(2,1)}), bf16[256,8,128]{2,0,1:T(8,128)(2,1)S(1)}, u32[]{:S(2)}, u32[]{:S(2)}) async-start(bf16[256,8,128]{2,0,1:T(8,128)(2,1)} %bitcast.22), calls=%async_computation.1 | async-start | bytes 1048576 | tf_op jit(solution)/shard_map/all_to_all | solution.py:113
  22.3 11.9 %all-to-all-done.1 = bf16[256,8,128]{2,0,1:T(8,128)(2,1)S(1)} async-done(((bf16[256,8,128]{2,0,1:T(8,128)(2,1)}), bf16[256,8,128]{2,0,1:T(8,128)(2,1)S(1)}, u32[]{:S(2)}, u32[]{:S(2)}) %all-to-all-start.1) | async-done | bytes 524320 | tf_op jit(solution)/shard_map/all_to_all | solution.py:113
  34.2 3.6 %all-to-all-start = ((bf16[256,16,128]{0,2,1:T(8,128)(2,1)}), bf16[256,16,128]{0,2,1:T(8,128)(2,1)S(1)}, u32[]{:S(2)}, u32[]{:S(2)}) async-start(bf16[256,16,128]{0,2,1:T(8,128)(2,1)} %pad_maximum_fusion), calls=%async_computation | async-start | bytes 2097152 | tf_op jit(solution)/shard_map/all_to_all | solution.py:112
  38.7 25.1 %all-to-all-done = bf16[256,16,128]{0,2,1:T(8,128)(2,1)S(1)} async-done(((bf16[256,16,128]{0,2,1:T(8,128)(2,1)}), bf16[256,16,128]{0,2,1:T(8,128)(2,1)S(1)}, u32[]{:S(2)}, u32[]{:S(2)}) %all-to-all-start) | async-done | bytes 1048608 | tf_op jit(solution)/shard_map/all_to_all | solution.py:112
  64.7 3.6 %all-to-all-start.2 = ((bf16[256,8,128]{2,0,1:T(8,128)(2,1)}), bf16[256,8,128]{2,0,1:T(8,128)(2,1)S(1)}, u32[]{:S(2)}, u32[]{:S(2)}) async-start(bf16[256,8,128]{2,0,1:T(8,128)(2,1)} %bitcast.26), calls=%async_computation.2 | async-start | bytes 1048576 | tf_op jit(solution)/shard_map/all_to_all | solution.py:114
  69.0 14.0 %all-to-all-done.2 = bf16[256,8,128]{2,0,1:T(8,128)(2,1)S(1)} async-done(((bf16[256,8,128]{2,0,1:T(8,128)(2,1)}), bf16[256,8,128]{2,0,1:T(8,128)(2,1)S(1)}, u32[]{:S(2)}, u32[]{:S(2)}) %all-to-all-start.2) | async-done | bytes 524320 | tf_op jit(solution)/shard_map/all_to_all | solution.py:114
  83.0 22.7 %while.10 = (s32[]{:T(128)}, bf16[4,512,1,2,128]{4,1,0,3,2:T(8,128)(2,1)}, bf16[4,512,1,2,128]{4,1,0,3,2:T(8,128)(2,1)S(1)}, bf16[2048,1,128]{2,0,1:T(8,128)(2,1...) while((s32[]{:T(128)}, bf16[4,512,1,2,128]{4,1,0,3,2:T(8,128)(2,1)}, ...), condition=%wide.region_5.6_spmd, body=%wide.region_2.5_spmd.sunk | while | flops 1092745216 | bytes 26759752 | solution.py:67
  83.0 1.3 bitcast_reduce_fusion.2
  84.3 1.6 fusion.63
  86.0 2.7 fusion.64
  90.0 1.6 fusion.63
  91.7 2.7 fusion.64
  95.7 1.6 fusion.63
  97.3 2.7 fusion.64
  100.0 1.3 bitcast_reduce_fusion.2
  101.4 1.6 fusion.63
  103.0 2.7 fusion.64
  105.7 3.7 %copy.124 = bf16[2048,2,128]{2,1,0:T(2,128)(2,1)} copy(bf16[2048,2,128]{2,0,1:T(8,128)(2,1)} %bitcast.160) | data formatting | bytes 2097152 | tf_op jit(solution)/shard_map/reshape | solution.py:67
  109.4 3.6 %all-to-all-start.3 = ((bf16[2048,2,128]{2,1,0:T(2,128)(2,1)}), bf16[2048,2,128]{2,1,0:T(2,128)(2,1)S(1)}, u32[]{:S(2)}, u32[]{:S(2)}) async-start(bf16[2048,2,128]{2,1,0:T(2,128)(2,1)} %copy.124), calls=%async_computation.3 | async-start | bytes 2097152 | tf_op jit(solution)/shard_map/all_to_all | solution.py:117
  115.4 2.6 scatter_custom_fusion
  118.0 21.0 %all-to-all-done.3 = bf16[2048,2,128]{2,1,0:T(2,128)(2,1)S(1)} async-done(((bf16[2048,2,128]{2,1,0:T(2,128)(2,1)}), bf16[2048,2,128]{2,1,0:T(2,128)(2,1)S(1)}, u32[]{:S(2)}, u32[]{:S(2)}) %all-to-all-start.3) | async-done | bytes 1048608 | tf_op jit(solution)/shard_map/all_to_all | solution.py:117
  139.7 5.9 %fusion.33 = (f32[256]{0:T(256)S(1)}, bf16[256,2048]{1,0:T(8,128)(2,1)S(1)}) fusion(bf16[256,2048]{0,1:T(8,128)(2,1)S(1)} %bitcast.153, bf16[2048,2048]{1,0:T(8,128)(2,1)} %all-gather.2.cloned.1.call-done, bf16[1,256,2048]{2,1,0:T(8,128)(2,1)S(1)} %copy-done.2), kind=kOutput, calls=%fused_computation.39 | convolution fusion | flops 2150629120 | bytes 11535360 | tf_op jit(solution)/shard_map/dot_general | solution.py:120
  147.0 4.3 %gather_fusion = bf16[768,2048]{1,0:T(8,128)(2,1)} fusion(bf16[257,2048]{1,0:T(8,128)(2,1)S(1)} %concatenate.13, s32[1024]{0:T(1024)S(1)} %pad_clamp_fusion.1), kind=kCustom, calls=%fused_computation | custom fusion | bytes 6294528 | tf_op jit(solution)/shard_map/gather | solution.py:143
  151.3 74.8 %all_to_all.76 = bf16[32,24,2048]{2,1,0:T(8,128)(2,1)S(1)} all-to-all(bf16[32,24,2048]{2,1,0:T(8,128)(2,1)} %bitcast.150), channel_id=1, replica_groups=mesh['sp'=8,'dp'=4] {'sp','dp'}, dimensions={0} | all-to-all | bytes 6291456 | tf_op jit(solution)/shard_map/all_to_all | solution.py:145
  226.1 3.4 %fusion.23 = f32[768,1024]{1,0:T(8,128)S(1)} fusion(bf16[768,2048]{1,0:T(8,128)(2,1)S(1)} %bitcast.158, bf16[1,2048,1024]{2,1,0:T(8,128)(2,1)S(1)} %copy-done.9), kind=kOutput, calls=%fused_computation.23 | convolution fusion | flops 3221225472 | bytes 10485760 | tf_op jit(solution)/shard_map/dot_general | solution.py:74
  229.6 4.1 %multiply_convert_fusion = bf16[768,1024]{1,0:T(8,128)(2,1)S(1)} fusion(f32[768,1024]{1,0:T(8,128)S(1)} %fusion.23, bf16[768,2048]{1,0:T(8,128)(2,1)S(1)} %bitcast.159, bf16[1,2048,1024]{2,1,0:T(8,128)(2,1)S(1)} %copy-done.10), kind=kOutput, calls=%fused_computation.29 | convolution fusion | flops 3229089792 | bytes 12058624 | tf_op jit(solution)/shard_map/dot_general | solution.py:72
  233.7 4.8 %fusion.27 = bf16[768,2048]{1,0:T(8,128)(2,1)} fusion(bf16[768,1024]{1,0:T(8,128)(2,1)S(1)} %multiply_convert_fusion, bf16[1,1024,2048]{2,1,0:T(8,128)(2,1)S(1)} %copy-done.11), kind=kOutput, calls=%fused_computation.28 | convolution fusion | flops 3222798336 | bytes 8912896 | tf_op jit(solution)/shard_map/dot_general | solution.py:78
  238.5 3.9 %all-to-all-start.5 = ((bf16[32,24,2048]{2,1,0:T(8,128)(2,1)}), bf16[32,24,2048]{2,1,0:T(8,128)(2,1)S(1)}, u32[]{:S(2)}, u32[]{:S(2)}) async-start(bf16[32,24,2048]{2,1,0:T(8,128)(2,1)} %bitcast.157), calls=%async_computation.5 | async-start | bytes 6291456 | tf_op jit(solution)/shard_map/all_to_all | solution.py:150
  242.6 71.2 %all-to-all-done.5 = bf16[32,24,2048]{2,1,0:T(8,128)(2,1)S(1)} async-done(((bf16[32,24,2048]{2,1,0:T(8,128)(2,1)}), bf16[32,24,2048]{2,1,0:T(8,128)(2,1)S(1)}, u32[]{:S(2)}, u32[]{:S(2)}) %all-to-all-start.5) | async-done | bytes 3145760 | tf_op jit(solution)/shard_map/all_to_all | solution.py:150
  313.8 3.3 gather_fusion.1
  317.1 5.4 %reshape.296 = f32[256,2,2048]{2,1,0:T(2,128)} reshape(bf16[512,2048]{1,0:T(8,128)(2,1)} %gather_fusion.1) | data formatting | bytes 6291456 | tf_op jit(solution)/shard_map/convert_element_type | solution.py:152
  322.6 9.0 %multiply_reduce_fusion = f32[256,2048]{1,0:T(8,128)S(1)} fusion(f32[256,2,2048]{2,1,0:T(2,128)} %reshape.296, f32[256,2]{1,0:T(8,128)S(1)} %copy.131), kind=kLoop, calls=%fused_computation.27 | loop fusion | flops 1572864 | bytes 6293504 | tf_op jit(solution)/shard_map/reduce_sum | solution.py:153
  (79 shorter events, 19.1 us)
Async XLA Ops:
  9.8 9.9 %copy-start.3 = (bf16[1,256,2048]{2,1,0:T(8,128)(2,1)S(1)}, bf16[1,256,2048]{2,1,0:T(8,128)(2,1)}, u32[]{:S(2)}) copy-start(bf16[1,256,2048]{2,1,0:T(8,128)(2,1)} %param.16) | copy-start | bytes 3145732
  10.7 9.8 %copy-start.8 = (f32[128]{0:T(128)S(1)}, f32[128]{0:T(128)}, u32[]{:S(2)}) copy-start(f32[128]{0:T(128)} %param.19) | copy-start | bytes 1540
  12.4 21.8 %all-to-all-start.1 = ((bf16[256,8,128]{2,0,1:T(8,128)(2,1)}), bf16[256,8,128]{2,0,1:T(8,128)(2,1)S(1)}, u32[]{:S(2)}, u32[]{:S(2)}) async-start(bf16[256,8,128]{2,0,1:T(8,128)(2,1)} %bitcast.22), calls=%async_computation.1 | async-start | bytes 1048576 | tf_op jit(solution)/shard_map/all_to_all | solution.py:113
  21.2 17.3 %copy-start.4 = (bf16[1,256,512]{2,1,0:T(8,128)(2,1)S(1)}, bf16[1,256,512]{2,1,0:T(8,128)(2,1)}, u32[]{:S(2)}) copy-start(bf16[1,256,512]{2,1,0:T(8,128)(2,1)} %param.18) | copy-start | bytes 786436
  34.2 29.6 %all-to-all-start = ((bf16[256,16,128]{0,2,1:T(8,128)(2,1)}), bf16[256,16,128]{0,2,1:T(8,128)(2,1)S(1)}, u32[]{:S(2)}, u32[]{:S(2)}) async-start(bf16[256,16,128]{0,2,1:T(8,128)(2,1)} %pad_maximum_fusion), calls=%async_computation | async-start | bytes 2097152 | tf_op jit(solution)/shard_map/all_to_all | solution.py:112
  37.8 101.9 %all-gather.2.cloned.1.call-start = ((), (), s32[]{:S(2)}) async-start(), calls=%async_computation.6 | async-start | bytes 10485760 | tf_op jit(solution)/shard_map/all_gather | solution.py:122
  64.7 18.3 %all-to-all-start.2 = ((bf16[256,8,128]{2,0,1:T(8,128)(2,1)}), bf16[256,8,128]{2,0,1:T(8,128)(2,1)S(1)}, u32[]{:S(2)}, u32[]{:S(2)}) async-start(bf16[256,8,128]{2,0,1:T(8,128)(2,1)} %bitcast.26), calls=%async_computation.2 | async-start | bytes 1048576 | tf_op jit(solution)/shard_map/all_to_all | solution.py:114
  105.7 7.3 %copy-start.6 = (s32[1,256,2]{1,2,0:T(2,128)S(1)}, s32[1,256,2]{1,2,0:T(2,128)}, u32[]{:S(2)}) copy-start(s32[1,256,2]{1,2,0:T(2,128)} %param.23) | copy-start | bytes 6148
  109.4 29.6 %all-to-all-start.3 = ((bf16[2048,2,128]{2,1,0:T(2,128)(2,1)}), bf16[2048,2,128]{2,1,0:T(2,128)(2,1)S(1)}, u32[]{:S(2)}, u32[]{:S(2)}) async-start(bf16[2048,2,128]{2,1,0:T(2,128)(2,1)} %copy.124), calls=%async_computation.3 | async-start | bytes 2097152 | tf_op jit(solution)/shard_map/all_to_all | solution.py:117
  113.0 26.7 %copy-start.2 = (bf16[1,256,2048]{2,1,0:T(8,128)(2,1)S(1)}, bf16[1,256,2048]{2,1,0:T(8,128)(2,1)}, u32[]{:S(2)}) copy-start(bf16[1,256,2048]{2,1,0:T(8,128)(2,1)} %param.15) | copy-start | bytes 3145732
  139.7 6.9 %copy-start.5 = (f32[2048]{0:T(1024)S(1)}, f32[2048]{0:T(1024)}, u32[]{:S(2)}) copy-start(f32[2048]{0:T(1024)} %param.22) | copy-start | bytes 24580
  145.6 1.0 copy-start
  151.3 74.8 %copy-start.9 = (bf16[1,2048,1024]{2,1,0:T(8,128)(2,1)S(1)}, bf16[1,2048,1024]{2,1,0:T(8,128)(2,1)}, u32[]{:S(2)}) copy-start(bf16[1,2048,1024]{2,1,0:T(8,128)(2,1)} %param.26) | copy-start | bytes 12582916
  226.1 3.5 %copy-start.10 = (bf16[1,2048,1024]{2,1,0:T(8,128)(2,1)S(1)}, bf16[1,2048,1024]{2,1,0:T(8,128)(2,1)}, u32[]{:S(2)}) copy-start(bf16[1,2048,1024]{2,1,0:T(8,128)(2,1)} %param.25) | copy-start | bytes 12582916
  229.6 4.2 %copy-start.11 = (bf16[1,1024,2048]{2,1,0:T(8,128)(2,1)S(1)}, bf16[1,1024,2048]{2,1,0:T(8,128)(2,1)}, u32[]{:S(2)}) copy-start(bf16[1,1024,2048]{2,1,0:T(8,128)(2,1)} %param.27) | copy-start | bytes 12582916
  238.5 3.9 %copy-start.7 = (f32[1,256,2]{1,2,0:T(2,128)S(1)}, f32[1,256,2]{1,2,0:T(2,128)}, u32[]{:S(2)}) copy-start(f32[1,256,2]{1,2,0:T(2,128)} %param.24) | copy-start | bytes 6148
  238.5 75.3 %all-to-all-start.5 = ((bf16[32,24,2048]{2,1,0:T(8,128)(2,1)}), bf16[32,24,2048]{2,1,0:T(8,128)(2,1)S(1)}, u32[]{:S(2)}, u32[]{:S(2)}) async-start(bf16[32,24,2048]{2,1,0:T(8,128)(2,1)} %bitcast.157), calls=%async_computation.5 | async-start | bytes 6291456 | tf_op jit(solution)/shard_map/all_to_all | solution.py:150
  322.6 9.0 %copy-start.1 = (bf16[256,2048]{1,0:T(8,128)(2,1)S(1)}, bf16[256,2048]{1,0:T(8,128)(2,1)}, u32[]{:S(2)}) copy-start(bf16[256,2048]{1,0:T(8,128)(2,1)} %copy-done) | copy-start | bytes 3145732
Sparse Core Ops, SparseCore 0:
  40.2 59.6 all-gather.1
where the time goes:
time: 340 us
  waiting for transfers between devices  144 us (42%)
  blocking collectives  74.8 us (22%)
  matrix products  34.4 us (10%)
  local copies, waits for them, and re-layouts  26.8 us (8%)
  other arithmetic  23.8 us (7%)
  starting transfers between devices  22.1 us (6%)
  between operations  13.8 us (4%)
    all_to_all x1, blocking collectives, per_device(): lax.all_to_all(outgoing, ('sp', 'dp'), split_axis=0, concat_axis=0, tiled...  74.8 us
    all_to_all x1, waiting for transfers between devices, per_device(): lax.all_to_all(answered, ('sp', 'dp'), split_axis=0, concat_axis=0, tiled...  71.2 us
    all_to_all x1, waiting for transfers between devices, per_device(): lax.all_to_all(query_turned, 'sp', split_axis=1, concat_axis=0, tiled=True)  25.1 us
    all_to_all x1, waiting for transfers between devices, per_device(): lax.all_to_all(head_out, 'sp', split_axis=0, concat_axis=1, tiled=True)  21 us
    all_to_all x1, waiting for transfers between devices, per_device(): lax.all_to_all(value_heads, 'sp', split_axis=1, concat_axis=0, tiled=True)  14 us
    all_to_all x1, waiting for transfers between devices, per_device(): lax.all_to_all(key_turned, 'sp', split_axis=1, concat_axis=0, tiled=True)  11.9 us
    dot_general x4, matrix products, one_block(): jnp.einsum('kgqs,skd->qkgd', attn_weights, head_value, preferred_element_...  10.8 us
    reduce_sum x1, other arithmetic, per_device(): jnp.sum(weighted.reshape(tok_rows, top_count, model_width), axis=1)  8.96 us
  transfers between devices with their start and end apart: 6, of which 5 were waited for; matrix products, arithmetic and copies ran while one was open for 11% of the time, Pallas kernels for 0%

commit v1 on v0

v1 whole, which is shorter than its diff:
```python
import functools

import jax
import jax.numpy as jnp
from jax import lax
from jax.experimental import pallas as pl
from jax.experimental.pallas import tpu as pltpu
from jax.sharding import PartitionSpec as P

GRID_W = 64
EPSILON = 1e-06
THETA = 10000.0
LIMIT = 7.0
SLOPE = 1.702
LOG2E = 1.4426950408889634
MESH = pl.DeviceIdType.MESH
VMEM_BYTES = 64000000


def split_of(count, inner):
    return (count // inner, inner) if count % inner == 0 else (count, 1)


def turn_tables(places, head_dim):
    quarter = head_dim // 4
    inverse = THETA ** (-jnp.arange(quarter, dtype=jnp.float32) / quarter)
    row = (places // GRID_W).astype(jnp.float32)[:, None] * inverse[None, :]
    col = (places % GRID_W).astype(jnp.float32)[:, None] * inverse[None, :]
    cosine = jnp.concatenate([jnp.cos(row)] * 2 + [jnp.cos(col)] * 2, axis=-1)
    sine = jnp.concatenate(
        [-jnp.sin(row), jnp.sin(row), -jnp.sin(col), jnp.sin(col)], axis=-1
    )
    return cosine, sine


def attention_kernel(
    planes, lanes_x, outer_dp, inner_dp,
    q_ref, k_ref, v_ref, qg_ref, kg_ref, cos_ref, sin_ref, resid_ref, ng_ref, w_ref,
    upd_ref, normed_ref,
    kall, vall, wall, qt, acc, mx, ls, head_out,
    kx_s, kx_r, kz_s, kz_r, vz_s, vz_r, vx_s, vx_r, wy_s, wy_r, wc_s, wc_r, loc,
):
    Z, X, Y, C = planes, lanes_x, outer_dp, inner_dp
    rows, head_dim = cos_ref.shape
    q_heads = q_ref.shape[1] // head_dim
    kv_heads = k_ref.shape[1] // head_dim
    group = q_heads // kv_heads
    w_rows = w_ref.shape[0]
    sp, dp = lax.axis_index("sp"), lax.axis_index("dp")
    z, x = sp // X, sp % X
    y, c = dp // C, dp % C
    up_ok, down_ok = z + 1 < Z, z > 0

    barrier = pltpu.get_barrier_semaphore()

    def greet(device):
        pl.semaphore_signal(barrier, inc=1, device_id=device, device_id_type=MESH)

    for j in range(1, X):
        greet((z * X + (x + j) % X, dp))

    @pl.when(up_ok)
    def _():
        greet((sp + X, dp))

    @pl.when(down_ok)
    def _():
        greet((sp - X, dp))

    for j in range(1, Y):
        greet((sp, ((y + j) % Y) * C + c))
    for j in range(1, C):
        greet((sp, y * C + (c + j) % C))

    def krows(block):
        return pl.ds(pl.multiple_of(block * rows, rows), rows)

    def wrows(block):
        return pl.ds(pl.multiple_of(block * w_rows, w_rows), w_rows)

    v_own = pltpu.make_async_copy(v_ref, vall.at[krows(sp)], loc.at[0])
    v_own.start()
    w_own = pltpu.make_async_copy(w_ref, wall.at[wrows(dp)], loc.at[1])
    w_own.start()

    lane = lax.broadcasted_iota(jnp.int32, (rows, head_dim), 1)
    first = lane % (head_dim // 2) < head_dim // 4

    def turned(value, gain):
        value = value.astype(jnp.float32)
        value = value * lax.rsqrt(jnp.mean(value * value, axis=-1, keepdims=True) + EPSILON) * gain
        swapped = jnp.where(
            first,
            pltpu.roll(value, head_dim - head_dim // 4, 1),
            pltpu.roll(value, head_dim // 4, 1),
        )
        return (value * cos_ref[...] + swapped * sin_ref[...]).astype(jnp.bfloat16)

    for g in range(kv_heads):
        span = slice(g * head_dim, (g + 1) * head_dim)
        kall[krows(sp), span] = turned(k_ref[:, span], kg_ref[...])

    count = (X - 1) + (Y - 1) + (C - 1) + up_ok.astype(jnp.int32) + down_ok.astype(jnp.int32)
    v_own.wait()
    w_own.wait()
    pl.semaphore_wait(barrier, count)

    def remote(buf, sl, ssem, rsem, device):
        return pltpu.make_async_remote_copy(
            src_ref=buf.at[sl], dst_ref=buf.at[sl], send_sem=ssem, recv_sem=rsem,
            device_id=device, device_id_type=MESH,
        )

    def kx(j):
        return remote(kall, krows(sp), kx_s.at[j], kx_r.at[j], (z * X + (x + j) % X, dp))

    def kz(d, s, j):
        plane = z - s if d == 0 else z + s
        device = (sp + X if d == 0 else sp - X, dp)
        at = (d * (Z - 1) + s) * X + j
        return remote(kall, krows(plane * X + (x + X - j) % X), kz_s.at[at], kz_r.at[at], device)

    def vz(d, s):
        plane = z - s if d == 0 else z + s
        device = (sp + X if d == 0 else sp - X, dp)
        at = d * (Z - 1) + s
        return remote(vall, krows(plane * X + x), vz_s.at[at], vz_r.at[at], device)

    def vx(slot, plane, j):
        at = slot * X + j
        return remote(
            vall, krows(plane * X + x), vx_s.at[at], vx_r.at[at], (z * X + (x + j) % X, dp)
        )

    def sends(d, s):
        if d == 0:
            return jnp.logical_and(up_ok, z - s >= 0)
        return jnp.logical_and(down_ok, z + s < Z)

    def gets(d, s):
        return z - s - 1 >= 0 if d == 0 else z + s + 1 < Z

    def wy(j):
        return remote(wall, wrows(dp), wy_s.at[j], wy_r.at[j], (sp, ((y + j) % Y) * C + c))

    def wc(j, i):
        at = j * C + i
        return remote(
            wall, wrows(((y + Y - j) % Y) * C + c), wc_s.at[at], wc_r.at[at],
            (sp, y * C + (c + i) % C),
        )

    for j in range(1, X):
        kx(j).start()
    for d in range(2):
        @pl.when(sends(d, 0))
        def _(d=d):
            kz(d, 0, 0).start()
            vz(d, 0).start()
    for j in range(1, X):
        vx(0, z, j).start()
    for j in range(1, Y):
        wy(j).start()
    for i in range(1, C):
        wc(0, i).start()

    def prepare_queries(h, carry):
        at = pl.ds(pl.multiple_of(h * head_dim, head_dim), head_dim)
        qt[h] = turned(q_ref[:, at], qg_ref[...])
        return carry

    lax.fori_loop(0, q_heads // 4, prepare_queries, 0)
    for j in range(1, X):
        kx(j).wait_recv()
    for d in range(2):
        @pl.when(sends(d, 0))
        def _(d=d):
            for j in range(1, X):
                kz(d, 0, j).start()
    lax.fori_loop(q_heads // 4, q_heads, prepare_queries, 0)

    factor = head_dim ** (-0.5) * LOG2E
    keys_in = X * rows

    def attend(plane, fresh):
        at_rows = pl.ds(pl.multiple_of(plane * keys_in, keys_in), keys_in)

        def pair(i, carry):
            for u in range(2):
                h = i * 2 + u
                span = pl.ds(pl.multiple_of((h // group) * head_dim, head_dim), head_dim)
                scores = lax.dot_general(
                    qt[h], kall[at_rows, span], (((1,), (1,)), ((), ())),
                    preferred_element_type=jnp.float32,
                )
                top = jnp.max(scores, axis=-1, keepdims=True)
                if not fresh:
                    before = mx[h]
                    top = jnp.maximum(before[:, :1], top)
                lifted = jnp.exp2((scores - top) * factor)
                total = jnp.sum(lifted, axis=-1, keepdims=True)
                part = jnp.dot(
                    lifted.astype(jnp.bfloat16), vall[at_rows, span],
                    preferred_element_type=jnp.float32,
                )
                wide = jnp.broadcast_to(top, (rows, head_dim))
                wide_total = jnp.broadcast_to(total, (rows, head_dim))
                if fresh:
                    acc[h], ls[h] = part, wide_total
                else:
                    fade = jnp.exp2((before - wide) * factor)
                    acc[h] = acc[h] * fade + part
                    ls[h] = ls[h] * fade + wide_total
                mx[h] = wide
            return carry

        lax.fori_loop(0, q_heads // 2, pair, 0)

    def wait_vx(slot, plane):
        for j in range(1, X):
            vx(slot, plane, j).wait_recv()

    def attend_step(s):
        def one(t, carry):
            plane = jnp.where(t == 0, z - s - 1, z + s + 1)

            @pl.when(jnp.logical_and(plane >= 0, plane < Z))
            def _():
                wait_vx(1 + s + t * (Z - 1), plane)
                attend(plane, False)
            return carry

        lax.fori_loop(0, 2, one, 0)

    for s in range(Z - 1):
        for d in range(2):
            @pl.when(gets(d, s))
            def _(d=d, s=s):
                plane = z - s - 1 if d == 0 else z + s + 1
                vz(d, s).wait_recv()
                for j in range(1, X):
                    vx(1 + s + d * (Z - 1), plane, j).start()
                if s + 1 < Z - 1:
                    @pl.when(sends(d, s + 1))
                    def _():
                        vz(d, s + 1).start()
                for j in range(X):
                    kz(d, s, j).wait_recv()
                    if s + 1 < Z - 1:
                        @pl.when(sends(d, s + 1))
                        def _(j=j):
                            kz(d, s + 1, j).start()
        if s == 0:
            wait_vx(0, z)
            attend(z, True)
        else:
            attend_step(s - 1)
        if s == 0:
            pass
    if Z == 1:
        wait_vx(0, z)
        attend(z, True)
    else:
        attend_step(Z - 2)

    for j in range(1, Y):
        wy(j).wait_recv()
        for i in range(1, C):
            wc(j, i).start()

    for h in range(q_heads):
        head_out[:, h * head_dim:(h + 1) * head_dim] = (acc[h] / ls[h]).astype(jnp.bfloat16)

    for j in range(Y):
        for i in range(1, C):
            wc(j, i).wait_recv()

    width = wall.shape[1]
    tile = min(256, width)

    def project(n, total):
        at = pl.ds(pl.multiple_of(n * tile, tile), tile)
        projected = jnp.dot(head_out[...], wall[:, at], preferred_element_type=jnp.float32)
        updated = (resid_ref[:, at].astype(jnp.float32) + projected).astype(jnp.bfloat16)
        upd_ref[:, at] = updated
        wide = updated.astype(jnp.float32)
        return total + jnp.sum(wide * wide, axis=-1, keepdims=True)

    square = lax.fori_loop(0, width // tile, project, jnp.zeros((rows, 1), jnp.float32))
    scale = lax.rsqrt(square / width + EPSILON)

    def normalize(n, carry):
        at = pl.ds(pl.multiple_of(n * tile, tile), tile)
        normed_ref[:, at] = (
            upd_ref[:, at].astype(jnp.float32) * scale * ng_ref[:, at]
        ).astype(jnp.bfloat16)
        return carry

    lax.fori_loop(0, width // tile, normalize, 0)

    for j in range(1, X):
        kx(j).wait_send()
        vx(0, z, j).wait_send()
    for d in range(2):
        for s in range(Z - 1):
            @pl.when(sends(d, s))
            def _(d=d, s=s):
                vz(d, s).wait_send()
                for j in range(X):
                    kz(d, s, j).wait_send()

            @pl.when(gets(d, s))
            def _(d=d, s=s):
                plane = z - s - 1 if d == 0 else z + s + 1
                for j in range(1, X):
                    vx(1 + s + d * (Z - 1), plane, j).wait_send()
    for j in range(1, Y):
        wy(j).wait_send()
    for j in range(Y):
        for i in range(1, C):
            wc(j, i).wait_send()


def attention(query, keys, values, q_gain, k_gain, cosine, sine, resid, norm_gain, out_weight):
    sp_count, dp_count = lax.axis_size("sp"), lax.axis_size("dp")
    planes = 4 if sp_count % 4 == 0 else 1
    lanes_x = sp_count // planes
    outer_dp, inner_dp = split_of(dp_count, 2)
    rows, head_dim = cosine.shape
    q_heads = query.shape[1] // head_dim
    width = resid.shape[1]
    dma = pltpu.SemaphoreType.DMA
    vmem = pl.BlockSpec(memory_space=pltpu.VMEM)
    hops = 2 * max(planes - 1, 1)
    full_kv = (sp_count * rows, keys.shape[1])
    return pl.pallas_call(
        functools.partial(attention_kernel, planes, lanes_x, outer_dp, inner_dp),
        name="gathered_attention",
        out_shape=(
            jax.ShapeDtypeStruct((rows, width), jnp.bfloat16),
            jax.ShapeDtypeStruct((rows, width), jnp.bfloat16),
        ),
        in_specs=[vmem, vmem, pl.BlockSpec(memory_space=pl.ANY)]
        + [vmem] * 6
        + [pl.BlockSpec(memory_space=pl.ANY)],
        out_specs=(vmem, vmem),
        scratch_shapes=[
            pltpu.VMEM(full_kv, jnp.bfloat16),
            pltpu.VMEM(full_kv, jnp.bfloat16),
            pltpu.VMEM((dp_count * out_weight.shape[0], width), jnp.bfloat16),
            pltpu.VMEM((q_heads, rows, head_dim), jnp.bfloat16),
            pltpu.VMEM((q_heads, rows, head_dim), jnp.float32),
            pltpu.VMEM((q_heads, rows, head_dim), jnp.float32),
            pltpu.VMEM((q_heads, rows, head_dim), jnp.float32),
            pltpu.VMEM((rows, q_heads * head_dim), jnp.bfloat16),
            dma((lanes_x,)), dma((lanes_x,)),
            dma((hops * lanes_x,)), dma((hops * lanes_x,)),
            dma((hops,)), dma((hops,)),
            dma(((hops + 1) * lanes_x,)), dma(((hops + 1) * lanes_x,)),
            dma((outer_dp,)), dma((outer_dp,)),
            dma((outer_dp * inner_dp,)), dma((outer_dp * inner_dp,)),
            dma((2,)),
        ],
        compiler_params=pltpu.CompilerParams(
            collective_id=0, has_side_effects=True, vmem_limit_bytes=VMEM_BYTES
        ),
    )(
        query, keys, values, q_gain[None], k_gain[None], cosine, sine, resid,
        norm_gain[None], out_weight,
    )


def apply_expert(batch, gate_matrix, up_matrix, down_matrix):
    flat_rows = batch.reshape(-1, batch.shape[-1])
    gated = jnp.minimum(jnp.dot(flat_rows, gate_matrix, preferred_element_type=jnp.float32), LIMIT)
    linear = jnp.clip(
        jnp.dot(flat_rows, up_matrix, preferred_element_type=jnp.float32), -LIMIT, LIMIT
    )
    active = (gated * jax.nn.sigmoid(SLOPE * gated) * (linear + 1.0)).astype(jnp.bfloat16)
    return (
        jnp.dot(active, down_matrix, preferred_element_type=jnp.float32)
        .astype(jnp.bfloat16)
        .reshape(batch.shape)
    )


def per_device(
    resid,
    query,
    keys,
    values,
    q_gain,
    k_gain,
    out_weight,
    norm_gain,
    route_ids,
    route_weight,
    expert_gate,
    expert_up,
    expert_down,
):
    span_devices = lax.axis_size("sp")
    experts_total = span_devices * lax.axis_size("dp")
    tok_rows = resid.shape[1]
    model_width = resid.shape[2]
    head_dim = q_gain.shape[0]
    places = lax.axis_index("sp") * tok_rows + jnp.arange(tok_rows, dtype=jnp.int32)
    cosine, sine = turn_tables(places, head_dim)
    updated, normed = attention(
        query[0], keys[0], values[0], q_gain, k_gain, cosine, sine, resid[0], norm_gain, out_weight
    )
    widened = updated.astype(jnp.float32)
    top_count = route_ids.shape[2]
    capacity = max(2, 3 * tok_rows * top_count // (2 * experts_total))
    chosen = route_ids[0].reshape(-1)
    onehot = (chosen[:, None] == jnp.arange(experts_total, dtype=jnp.int32)[None, :]).astype(
        jnp.int32
    )
    earlier = jnp.sum((jnp.cumsum(onehot, axis=0) - onehot) * onehot, axis=1)
    target = chosen * capacity + earlier
    sources = jnp.arange(tok_rows * top_count, dtype=jnp.int32) // top_count
    slot_table = jnp.full((experts_total * capacity,), tok_rows, jnp.int32).at[target].set(sources)
    padded = jnp.concatenate([normed, jnp.zeros((1, model_width), jnp.bfloat16)], axis=0)
    outgoing = padded[slot_table].reshape(experts_total, capacity, model_width)
    answered = apply_expert(
        lax.all_to_all(outgoing, ("sp", "dp"), split_axis=0, concat_axis=0, tiled=True),
        expert_gate[0],
        expert_up[0],
        expert_down[0],
    )
    returned = lax.all_to_all(answered, ("sp", "dp"), split_axis=0, concat_axis=0, tiled=True)
    results = returned.reshape(experts_total * capacity, model_width)[target]
    weighted = results.astype(jnp.float32) * route_weight[0].reshape(-1)[:, None]
    combined = jnp.sum(weighted.reshape(tok_rows, top_count, model_width), axis=1)
    return (widened + combined).astype(jnp.bfloat16)[None]


def solution(mesh):
    placed = (
        P("dp", "sp", None),
        P("dp", "sp", None),
        P("dp", "sp", None),
        P("dp", "sp", None),
        P(),
        P(),
        P("dp", None),
        P(),
        P("dp", "sp", None),
        P("dp", "sp", None),
        P(("sp", "dp"), None, None),
        P(("sp", "dp"), None, None),
        P(("sp", "dp"), None, None),
    )
    return jax.shard_map(
        per_device, mesh=mesh, in_specs=placed, out_specs=P("dp", "sp", None), check_vma=False
    )
```

time: 340 us -> 282 us (0.83)
  Pallas kernels: 0 us -> 82.8 us
  waiting for transfers between devices: 144 us -> 71.2 us
  matrix products: 34.4 us -> 12.4 us
  starting transfers between devices: 22.1 us -> 3.88 us
  between operations: 13.8 us -> 0.18 us
  other arithmetic: 23.8 us -> 14.9 us
  local copies, waits for them, and re-layouts: 26.8 us -> 18.5 us
    pallas_call x0 -> x1, Pallas kernels: none -> 82.8 us  [attention(): pl.pallas_call(functools.partial(attention_kernel, planes, lanes_x, outer...]
    all_to_all x4 -> x0, waiting for transfers between devices: 72 us -> none  [the longest x1 25.1 us: per_device(): lax.all_to_all(query_turned, 'sp', split_axis=1, concat_axis=0, tiled=True)]
    dot_general x9 -> x0, matrix products: 22 us -> none  [the longest x4 10.8 us: one_block(): jnp.einsum('kgqs,skd->qkgd', attn_weights, head_value, preferred_element_...]
    all_to_all x4 -> x0, starting transfers between devices: 18.2 us -> none  [the longest x1 7.28 us: per_device(): lax.all_to_all(key_turned, 'sp', split_axis=1, concat_axis=0, tiled=True)]
    reduce_sum x6 -> x0, other arithmetic: 7.13 us -> none  [the longest x4 6.56 us: one_block(): jnp.sum(lifted, axis=-1, keepdims=True)]
    reshape x1 -> x0, local copies, waits for them, and re-layouts: 3.7 us -> none  [attend(): lax.map(one_block, query_blocks).reshape(length, local_heads, head_dim)]
  transfers between devices with their start and end apart: 6 -> 1, of which waited for: 5 -> 1; matrix products, arithmetic and copies ran while one was open for 11% -> 0% of each run, Pallas kernels for 0% -> 0%
where the time goes in v1:
time: 282 us; the launch traced here: 281 us
  Pallas kernels  82.8 us (29%)
  blocking collectives  77.5 us (27%)
  waiting for transfers between devices  71.2 us (25%)
  local copies, waits for them, and re-layouts  18.5 us (7%)
  other arithmetic  14.9 us (5%)
  matrix products  12.4 us (4%)
  starting transfers between devices  3.88 us (1%)
    pallas_call x1, Pallas kernels, attention(): pl.pallas_call(functools.partial(attention_kernel, planes, lanes_x, outer...  82.8 us
    all_to_all x1, blocking collectives, per_device(): lax.all_to_all(outgoing, ('sp', 'dp'), split_axis=0, concat_axis=0, tiled...  77.5 us
    all_to_all x1, waiting for transfers between devices, per_device(): lax.all_to_all(answered, ('sp', 'dp'), split_axis=0, concat_axis=0, tiled...  71.2 us
    reduce_sum x1, other arithmetic, per_device(): jnp.sum(weighted.reshape(tok_rows, top_count, model_width), axis=1)  8.96 us
  transfers between devices with their start and end apart: 1, of which 1 were waited for; matrix products, arithmetic and copies ran while one was open for 0% of the time, Pallas kernels for 0%

profile of v1, /device:TPU:0, one launch (start us, length us, event | category | flops | bytes accessed | tf_op | source)
XLA Modules:
  0.0 281.4 jit_solution(5531556987439603416)
XLA Ops:
  0.0 0.8 copy.23
  0.8 0.1 eq.31
  1.0 0.1 eq.27
  1.1 0.7 broadcast_multiply_fusion
  1.8 1.2 reduce-window.6
  3.0 0.2 slice_reduce_fusion
  3.3 0.1 copy.22
  3.4 0.1 mul.79
  3.6 0.1 fusion.14
  3.7 2.4 scatter_custom_fusion
  6.2 1.0 fusion.16
  7.2 0.8 pad_maximum_fusion.cos_ref
  8.0 0.8 pad_maximum_fusion.1.sin_ref
  8.8 82.8 %gathered_attention.1 = (bf16[256,2048]{1,0:T(8,128)(2,1)}, bf16[256,2048]{1,0:T(8,128)(2,1)}) custom-call(bf16[256,2048]{1,0:T(8,128)(2,1)} %bitcast.56, bf16[256,512]{1,0:T(8,128)(2,1)} %bitcast.58, bf16[256,512]{1,0:T(8,128)(2,1)} %bitcast.59, f32[1,128]{1,0:T(1,128)} %bitcast.65, f32[1,128]{1,0:T(1,128)} %bitcast.66, ...), custom_call_target="tpu_custom_call" | custom-call | tf_op jit(solution)/shard_map/gathered_attention/pallas_call | solution.py:336
  91.6 1.3 concatenate.11
  92.9 4.3 %gather_fusion = bf16[768,2048]{1,0:T(8,128)(2,1)} fusion(bf16[257,2048]{1,0:T(8,128)(2,1)S(1)} %concatenate.11, s32[1024]{0:T(1024)S(1)} %pad_clamp_fusion.1), kind=kCustom, calls=%fused_computation | custom fusion | bytes 6294528 | tf_op jit(solution)/shard_map/gather | solution.py:424
  97.2 77.5 %all_to_all.10 = bf16[32,24,2048]{2,1,0:T(8,128)(2,1)S(1)} all-to-all(bf16[32,24,2048]{2,1,0:T(8,128)(2,1)} %bitcast.52), channel_id=1, replica_groups=mesh['sp'=8,'dp'=4] {'sp','dp'}, dimensions={0} | all-to-all | bytes 6291456 | tf_op jit(solution)/shard_map/all_to_all | solution.py:426
  174.7 0.0 copy-done.2
  174.7 3.4 %fusion.2 = f32[768,1024]{1,0:T(8,128)S(1)} fusion(bf16[768,2048]{1,0:T(8,128)(2,1)S(1)} %bitcast.54, bf16[1,2048,1024]{2,1,0:T(8,128)(2,1)S(1)} %copy-done.2), kind=kOutput, calls=%fused_computation.5 | convolution fusion | flops 3221225472 | bytes 10485760 | tf_op jit(solution)/shard_map/dot_general | solution.py:377
  178.1 0.0 copy-done.3
  178.1 0.0 copy-start.4
  178.2 4.1 %multiply_convert_fusion = bf16[768,1024]{1,0:T(8,128)(2,1)S(1)} fusion(f32[768,1024]{1,0:T(8,128)S(1)} %fusion.2, bf16[768,2048]{1,0:T(8,128)(2,1)S(1)} %bitcast.55, bf16[1,2048,1024]{2,1,0:T(8,128)(2,1)S(1)} %copy-done.3), kind=kOutput, calls=%fused_computation.11 | convolution fusion | flops 3229089792 | bytes 12058624 | tf_op jit(solution)/shard_map/dot_general | solution.py:375
  182.3 0.0 copy-done.4
  182.3 4.8 %fusion.6 = bf16[768,2048]{1,0:T(8,128)(2,1)} fusion(bf16[768,1024]{1,0:T(8,128)(2,1)S(1)} %multiply_convert_fusion, bf16[1,1024,2048]{2,1,0:T(8,128)(2,1)S(1)} %copy-done.4), kind=kOutput, calls=%fused_computation.10 | convolution fusion | flops 3222798336 | bytes 8912896 | tf_op jit(solution)/shard_map/dot_general | solution.py:381
  187.1 3.9 %all-to-all-start.1 = ((bf16[32,24,2048]{2,1,0:T(8,128)(2,1)}), bf16[32,24,2048]{2,1,0:T(8,128)(2,1)S(1)}, u32[]{:S(2)}, u32[]{:S(2)}) async-start(bf16[32,24,2048]{2,1,0:T(8,128)(2,1)} %bitcast.53), calls=%async_computation.1 | async-start | bytes 6291456 | tf_op jit(solution)/shard_map/all_to_all | solution.py:431
  191.0 0.0 copy-done.1
  191.0 0.1 copy.26
  191.2 71.2 %all-to-all-done.1 = bf16[32,24,2048]{2,1,0:T(8,128)(2,1)S(1)} async-done(((bf16[32,24,2048]{2,1,0:T(8,128)(2,1)}), bf16[32,24,2048]{2,1,0:T(8,128)(2,1)S(1)}, u32[]{:S(2)}, u32[]{:S(2)}) %all-to-all-start.1) | async-done | bytes 3145760 | tf_op jit(solution)/shard_map/all_to_all | solution.py:431
  262.4 3.3 %gather_fusion.1 = bf16[512,2048]{1,0:T(8,128)(2,1)} fusion(bf16[768,2048]{1,0:T(8,128)(2,1)S(1)} %bitcast.51, s32[1024]{0:T(1024)S(1)} %pad_clamp_fusion), kind=kCustom, calls=%fused_computation.1 | custom fusion | bytes 4196352 | tf_op jit(solution)/shard_map/gather | solution.py:432
  265.7 5.4 %reshape.112 = f32[256,2,2048]{2,1,0:T(2,128)} reshape(bf16[512,2048]{1,0:T(8,128)(2,1)} %gather_fusion.1) | data formatting | bytes 6291456 | tf_op jit(solution)/shard_map/convert_element_type | solution.py:433
  271.2 9.0 %multiply_reduce_fusion = f32[256,2048]{1,0:T(8,128)S(1)} fusion(f32[256,2,2048]{2,1,0:T(2,128)} %reshape.112, f32[256,2]{1,0:T(8,128)S(1)} %copy.26), kind=kLoop, calls=%fused_computation.9 | loop fusion | flops 1572864 | bytes 6293504 | tf_op jit(solution)/shard_map/reduce_sum | solution.py:434
  280.1 1.3 fusion.11
  (15 shorter events, 0.1 us)
Async XLA Ops:
  97.2 77.5 %copy-start.2 = (bf16[1,2048,1024]{2,1,0:T(8,128)(2,1)S(1)}, bf16[1,2048,1024]{2,1,0:T(8,128)(2,1)}, u32[]{:S(2)}) copy-start(bf16[1,2048,1024]{2,1,0:T(8,128)(2,1)} %param.24) | copy-start | bytes 12582916
  174.7 3.5 %copy-start.3 = (bf16[1,2048,1024]{2,1,0:T(8,128)(2,1)S(1)}, bf16[1,2048,1024]{2,1,0:T(8,128)(2,1)}, u32[]{:S(2)}) copy-start(bf16[1,2048,1024]{2,1,0:T(8,128)(2,1)} %param.23) | copy-start | bytes 12582916
  178.1 4.2 %copy-start.4 = (bf16[1,1024,2048]{2,1,0:T(8,128)(2,1)S(1)}, bf16[1,1024,2048]{2,1,0:T(8,128)(2,1)}, u32[]{:S(2)}) copy-start(bf16[1,1024,2048]{2,1,0:T(8,128)(2,1)} %param.25) | copy-start | bytes 12582916
  187.1 3.9 %copy-start.1 = (f32[1,256,2]{1,2,0:T(2,128)S(1)}, f32[1,256,2]{1,2,0:T(2,128)}, u32[]{:S(2)}) copy-start(f32[1,256,2]{1,2,0:T(2,128)} %param.22) | copy-start | bytes 6148
  187.1 75.3 %all-to-all-start.1 = ((bf16[32,24,2048]{2,1,0:T(8,128)(2,1)}), bf16[32,24,2048]{2,1,0:T(8,128)(2,1)S(1)}, u32[]{:S(2)}, u32[]{:S(2)}) async-start(bf16[32,24,2048]{2,1,0:T(8,128)(2,1)} %bitcast.53), calls=%async_computation.1 | async-start | bytes 6291456 | tf_op jit(solution)/shard_map/all_to_all | solution.py:431
  271.2 9.0 %copy-start = (bf16[256,2048]{1,0:T(8,128)(2,1)S(1)}, bf16[256,2048]{1,0:T(8,128)(2,1)}, u32[]{:S(2)}) copy-start(bf16[256,2048]{1,0:T(8,128)(2,1)} %get-tuple-element.7) | copy-start | bytes 3145732

commit v2 on v1

--- a/solution.py
+++ b/solution.py
@@ -185,10 +185,10 @@
     def attend(plane, fresh):
         at_rows = pl.ds(pl.multiple_of(plane * keys_in, keys_in), keys_in)
 
-        def pair(i, carry):
-            for u in range(2):
-                h = i * 2 + u
-                span = pl.ds(pl.multiple_of((h // group) * head_dim, head_dim), head_dim)
+        def one_group(i, carry):
+            span = pl.ds(pl.multiple_of(i * head_dim, head_dim), head_dim)
+            for u in range(group):
+                h = i * group + u
                 scores = lax.dot_general(
                     qt[h], kall[at_rows, span], (((1,), (1,)), ((), ())),
                     preferred_element_type=jnp.float32,
@@ -214,7 +214,7 @@
                 mx[h] = wide
             return carry
 
-        lax.fori_loop(0, q_heads // 2, pair, 0)
+        lax.fori_loop(0, kv_heads, one_group, 0)
 
     def wait_vx(slot, plane):
         for j in range(1, X):
@@ -255,18 +255,16 @@
             attend(z, True)
         else:
             attend_step(s - 1)
-        if s == 0:
-            pass
+
+    for j in range(1, Y):
+        wy(j).wait_recv()
+        for i in range(1, C):
+            wc(j, i).start()
     if Z == 1:
         wait_vx(0, z)
         attend(z, True)
     else:
         attend_step(Z - 2)
-
-    for j in range(1, Y):
-        wy(j).wait_recv()
-        for i in range(1, C):
-            wc(j, i).start()
 
     for h in range(q_heads):
         head_out[:, h * head_dim:(h + 1) * head_dim] = (acc[h] / ls[h]).astype(jnp.bfloat16)
@@ -429,9 +427,12 @@
         expert_down[0],
     )
     returned = lax.all_to_all(answered, ("sp", "dp"), split_axis=0, concat_axis=0, tiled=True)
-    results = returned.reshape(experts_total * capacity, model_width)[target]
-    weighted = results.astype(jnp.float32) * route_weight[0].reshape(-1)[:, None]
-    combined = jnp.sum(weighted.reshape(tok_rows, top_count, model_width), axis=1)
+    rows_back = returned.reshape(experts_total * capacity, model_width)
+    slots = target.reshape(tok_rows, top_count)
+    combined = sum(
+        rows_back[slots[:, i]].astype(jnp.float32) * route_weight[0, :, i][:, None]
+        for i in range(top_count)
+    )
     return (widened + combined).astype(jnp.bfloat16)[None]
 
 

time: 282 us -> 265 us (0.940)
  other arithmetic: 14.9 us -> 7.64 us
  local copies, waits for them, and re-layouts: 18.5 us -> 14.3 us
  Pallas kernels: 82.8 us -> 79.6 us
    reduce_sum x1 -> x0, other arithmetic: 8.96 us -> none  [per_device(): jnp.sum(weighted.reshape(tok_rows, top_count, model_width), axis=1)]
    convert_element_type x1 -> x0, local copies, waits for them, and re-layouts: 5.44 us -> none  [per_device(): results.astype(jnp.float32) * route_weight[0].reshape(-1)[:, None]]
    pallas_call x1, Pallas kernels: 82.8 us -> 79.6 us  [attention(): pl.pallas_call(functools.partial(attention_kernel, planes, lanes_x, outer...]
where the time goes in v2:
time: 265 us
  Pallas kernels  79.6 us (30%)
  blocking collectives  75.9 us (29%)
  waiting for transfers between devices  71.2 us (27%)
  local copies, waits for them, and re-layouts  14.3 us (5%)
  matrix products  12.4 us (5%)
  other arithmetic  7.64 us (3%)
  starting transfers between devices  3.66 us (1%)
    pallas_call x1, Pallas kernels, attention(): pl.pallas_call(functools.partial(attention_kernel, planes, lanes_x, outer...  79.6 us
    all_to_all x1, blocking collectives, per_device(): lax.all_to_all(outgoing, ('sp', 'dp'), split_axis=0, concat_axis=0, tiled...  75.9 us
    all_to_all x1, waiting for transfers between devices, per_device(): lax.all_to_all(answered, ('sp', 'dp'), split_axis=0, concat_axis=0, tiled...  71.2 us
  transfers between devices with their start and end apart: 1, of which 1 were waited for; matrix products, arithmetic and copies ran while one was open for 0% of the time, Pallas kernels for 0%

profile of v2, /device:TPU:0, one launch (start us, length us, event | category | flops | bytes accessed | tf_op | source)
XLA Modules:
  0.0 264.9 jit_solution(15097267421758312239)
XLA Ops:
  0.0 0.8 copy.24
  0.8 0.1 eq.31
  1.0 0.1 eq.27
  1.2 1.2 reduce-window.6
  2.4 0.2 slice_reduce_fusion
  2.6 0.1 mul.92
  2.8 0.1 fusion.16
  2.9 2.4 scatter_custom_fusion
  5.4 1.0 fusion.18
  6.4 0.8 pad_maximum_fusion.cos_ref
  7.2 0.8 pad_maximum_fusion.1.sin_ref
  8.0 79.6 %gathered_attention.1 = (bf16[256,2048]{1,0:T(8,128)(2,1)}, bf16[256,2048]{1,0:T(8,128)(2,1)}) custom-call(bf16[256,2048]{1,0:T(8,128)(2,1)} %bitcast.61, bf16[256,512]{1,0:T(8,128)(2,1)} %bitcast.63, bf16[256,512]{1,0:T(8,128)(2,1)} %bitcast.64, f32[1,128]{1,0:T(1,128)} %bitcast.70, f32[1,128]{1,0:T(1,128)} %bitcast.71, ...), custom_call_target="tpu_custom_call" | custom-call | tf_op jit(solution)/shard_map/gathered_attention/pallas_call | solution.py:334
  87.6 1.3 concatenate.11
  88.9 4.3 %gather_fusion = bf16[768,2048]{1,0:T(8,128)(2,1)} fusion(bf16[257,2048]{1,0:T(8,128)(2,1)S(1)} %concatenate.11, s32[1024]{0:T(1024)S(1)} %pad_clamp_fusion.2), kind=kCustom, calls=%fused_computation | custom fusion | bytes 6294528 | tf_op jit(solution)/shard_map/gather | solution.py:422
  93.2 0.0 copy-start.1
  93.2 75.9 %all_to_all.10 = bf16[32,24,2048]{2,1,0:T(8,128)(2,1)S(1)} all-to-all(bf16[32,24,2048]{2,1,0:T(8,128)(2,1)} %bitcast.57), channel_id=1, replica_groups=mesh['sp'=8,'dp'=4] {'sp','dp'}, dimensions={0} | all-to-all | bytes 6291456 | tf_op jit(solution)/shard_map/all_to_all | solution.py:424
  169.1 0.0 copy-done.1
  169.1 0.0 copy-start.2
  169.1 3.4 %fusion.2 = f32[768,1024]{1,0:T(8,128)S(1)} fusion(bf16[768,2048]{1,0:T(8,128)(2,1)S(1)} %bitcast.59, bf16[1,2048,1024]{2,1,0:T(8,128)(2,1)S(1)} %copy-done.1), kind=kOutput, calls=%fused_computation.6 | convolution fusion | flops 3221225472 | bytes 10485760 | tf_op jit(solution)/shard_map/dot_general | solution.py:375
  172.5 0.0 copy-done.2
  172.5 0.0 copy-start.3
  172.5 4.1 %multiply_convert_fusion = bf16[768,1024]{1,0:T(8,128)(2,1)S(1)} fusion(f32[768,1024]{1,0:T(8,128)S(1)} %fusion.2, bf16[768,2048]{1,0:T(8,128)(2,1)S(1)} %bitcast.60, bf16[1,2048,1024]{2,1,0:T(8,128)(2,1)S(1)} %copy-done.2), kind=kOutput, calls=%fused_computation.11 | convolution fusion | flops 3229089792 | bytes 12058624 | tf_op jit(solution)/shard_map/dot_general | solution.py:373
  176.7 0.0 copy-done.3
  176.7 4.8 %fusion.6 = bf16[768,2048]{1,0:T(8,128)(2,1)} fusion(bf16[768,1024]{1,0:T(8,128)(2,1)S(1)} %multiply_convert_fusion, bf16[1,1024,2048]{2,1,0:T(8,128)(2,1)S(1)} %copy-done.3), kind=kOutput, calls=%fused_computation.10 | convolution fusion | flops 3222798336 | bytes 8912896 | tf_op jit(solution)/shard_map/dot_general | solution.py:379
  181.5 3.7 %all-to-all-start.1 = ((bf16[32,24,2048]{2,1,0:T(8,128)(2,1)}), bf16[32,24,2048]{2,1,0:T(8,128)(2,1)S(1)}, u32[]{:S(2)}, u32[]{:S(2)}) async-start(bf16[32,24,2048]{2,1,0:T(8,128)(2,1)} %bitcast.58), calls=%async_computation.1 | async-start | bytes 6291456 | tf_op jit(solution)/shard_map/all_to_all | solution.py:429
  185.2 0.1 reduce_sum.15
  185.3 0.2 fusion.12
  185.6 0.0 copy-done
  185.6 71.2 %all-to-all-done.1 = bf16[32,24,2048]{2,1,0:T(8,128)(2,1)S(1)} async-done(((bf16[32,24,2048]{2,1,0:T(8,128)(2,1)}), bf16[32,24,2048]{2,1,0:T(8,128)(2,1)S(1)}, u32[]{:S(2)}, u32[]{:S(2)}) %all-to-all-start.1) | async-done | bytes 3145760 | tf_op jit(solution)/shard_map/all_to_all | solution.py:429
  256.8 2.3 gather_fusion.2
  259.1 2.3 gather_fusion.1
  261.5 3.4 %fusion.11 = bf16[1,256,2048]{2,1,0:T(8,128)(2,1)} fusion(bf16[256,2048]{1,0:T(8,128)(2,1)} %gather_fusion.2, bf16[256,2048]{1,0:T(8,128)(2,1)} %gather_fusion.1, bf16[256,2048]{1,0:T(8,128)(2,1)} %get-tuple-element.7, f32[256]{0:T(256)S(1)} %bitcast.68, f32[256]{0:T(256)S(1)} %bitcast.67), kind=kLoop, calls=%fused_computation.13 | loop fusion | flops 4194304 | bytes 4196352 | tf_op jit(solution)/shard_map/broadcast_in_dim | solution.py:436
  (14 shorter events, 0.1 us)
Async XLA Ops:
  93.2 75.9 %copy-start.1 = (bf16[1,2048,1024]{2,1,0:T(8,128)(2,1)S(1)}, bf16[1,2048,1024]{2,1,0:T(8,128)(2,1)}, u32[]{:S(2)}) copy-start(bf16[1,2048,1024]{2,1,0:T(8,128)(2,1)} %param.24) | copy-start | bytes 12582916
  169.1 3.5 %copy-start.2 = (bf16[1,2048,1024]{2,1,0:T(8,128)(2,1)S(1)}, bf16[1,2048,1024]{2,1,0:T(8,128)(2,1)}, u32[]{:S(2)}) copy-start(bf16[1,2048,1024]{2,1,0:T(8,128)(2,1)} %param.23) | copy-start | bytes 12582916
  172.5 4.2 %copy-start.3 = (bf16[1,1024,2048]{2,1,0:T(8,128)(2,1)S(1)}, bf16[1,1024,2048]{2,1,0:T(8,128)(2,1)}, u32[]{:S(2)}) copy-start(bf16[1,1024,2048]{2,1,0:T(8,128)(2,1)} %param.25) | copy-start | bytes 12582916
  181.5 4.1 %copy-start = (f32[1,256,2]{1,2,0:T(2,128)S(1)}, f32[1,256,2]{1,2,0:T(2,128)}, u32[]{:S(2)}) copy-start(f32[1,256,2]{1,2,0:T(2,128)} %param.22) | copy-start | bytes 6148
  181.5 75.3 %all-to-all-start.1 = ((bf16[32,24,2048]{2,1,0:T(8,128)(2,1)}), bf16[32,24,2048]{2,1,0:T(8,128)(2,1)S(1)}, u32[]{:S(2)}, u32[]{:S(2)}) async-start(bf16[32,24,2048]{2,1,0:T(8,128)(2,1)} %bitcast.58), calls=%async_computation.1 | async-start | bytes 6291456 | tf_op jit(solution)/shard_map/all_to_all | solution.py:429
